TPU v7x, 512 devices: a whole 4x4x16 slice. The times are simulated.
512 devices in a mesh: sp: 16 (over z), dp: 32 (over y, x, core).
Axes of the slice: x: 4, y: 4, z: 16, core: 2. Of those that a mesh axis runs over, the one named last changes fastest.
Arguments:
- queries: bfloat16 [32, 2048, 1024], P('dp', 'sp'), may hold values from -6 to 6
- key_rows: bfloat16 [32, 2048, 1024], P('dp', 'sp'), may hold values from -6 to 6
- value_rows: bfloat16 [32, 2048, 1024], P('dp', 'sp'), may hold values from -6 to 6
- break_offset: bfloat16 [32, 2048, 16], P('dp', 'sp'), may hold values from 1.5 to 15
- hidden_in: bfloat16 [32, 2048, 2048], P('dp', 'sp'), may hold values from -6 to 6
- gate_weight: bfloat16 [2048, 1024], P('dp', 'sp'), may hold values from -0.125 to 0.125
- out_weight: bfloat16 [1024, 2048], P('sp', 'dp'), may hold values from -0.1875 to 0.1875
Outputs:
- mixed: bfloat16 [32, 2048, 2048], P('dp', 'sp')
All inputs are finite; a program needn't handle non-finite values.
Results may differ from a plain program's by a relative error of at most 0.0063.
Values may be sent and summed in bfloat16 or wider, within the bound.
No kernel may reach another device: no remote copies, remote signals or barrier semaphores. Data moves between devices by JAX's collectives and lax.ppermute only.
A program may use at most 64 MiB of HBM per device.

v0:
```python
import jax
import jax.numpy as jnp
from jax import lax
from jax.sharding import PartitionSpec as P

eps_norm = 1e-05


def turned_gather(arrays, axis, dims):
    turned = [jnp.moveaxis(a, dim, 0) for a, dim in zip(arrays, dims)]
    widths = [t[0].size for t in turned]
    both = jnp.concatenate([t.reshape(-1, w) for t, w in zip(turned, widths)], axis=1)
    out = lax.all_gather(both, axis, axis=0, tiled=True)
    blocks = jnp.split(out, [sum(widths[:k]) for k in range(1, len(widths))], axis=1)
    return tuple(
        (
            jnp.moveaxis(b.reshape(-1, *t.shape[1:]), 0, dim)
            for b, t, dim in zip(blocks, turned, dims)
        )
    )


def stick_blocks(head_queries, head_keys, head_values, head_offsets):
    groups, length, head_size = head_queries.shape
    block_rows = min(512, length)
    block_count = length // block_rows
    score_scale = head_size ** (-0.5)
    query_blocks = head_queries.reshape(groups, block_count, block_rows, head_size)

    def one_block(block_index):
        query_block = lax.dynamic_index_in_dim(query_blocks, block_index, 1, keepdims=False)
        query_pos = block_index * block_rows + jnp.arange(block_rows, dtype=jnp.int32)

        def key_step(step_turn, carry):
            running, carried = carry
            key_first = (block_index - step_turn) * block_rows
            key_block = lax.dynamic_slice_in_dim(head_keys, key_first, block_rows, 1)
            value_block = lax.dynamic_slice_in_dim(head_values, key_first, block_rows, 1)
            offset_block = lax.dynamic_slice_in_dim(head_offsets, key_first, block_rows, 1)
            scores = jnp.einsum(
                "gqd,gkd->gqk", query_block, key_block, preferred_element_type=jnp.float32
            )
            scores = scores * score_scale - offset_block[:, None, :]
            key_pos = key_first + jnp.arange(block_rows, dtype=jnp.int32)
            earlier = key_pos[None, :] < query_pos[:, None]
            keep_log = jnp.where(earlier, jax.nn.log_sigmoid(-scores), 0.0)
            later_sum = lax.cumsum(keep_log, axis=2, reverse=True) - keep_log + carried
            weights = jnp.where(
                earlier, jnp.exp(jax.nn.log_sigmoid(scores) + later_sum), 0.0
            ).astype(jnp.bfloat16)
            running = running + jnp.einsum(
                "gqk,gkd->gqd", weights, value_block, preferred_element_type=jnp.float32
            )
            carried = carried + jnp.sum(keep_log, axis=2, keepdims=True)
            return (running, carried)

        start_carry = (
            jnp.zeros((groups, block_rows, head_size), jnp.float32),
            jnp.zeros((groups, block_rows, 1), jnp.float32),
        )
        running, carried = lax.fori_loop(0, block_index + 1, key_step, start_carry)
        return running

    outputs = lax.map(one_block, jnp.arange(block_count, dtype=jnp.int32))
    return outputs.transpose(1, 0, 2, 3).reshape(groups, length, head_size)


def attend(pieces):
    head_queries, head_keys, head_values, head_offsets = pieces
    item_count, length, feature_count = head_queries.shape
    heads_dev = head_offsets.shape[2]
    head_size = feature_count // heads_dev

    def split_heads(array):
        return (
            array.reshape(item_count, length, heads_dev, head_size)
            .transpose(0, 2, 1, 3)
            .reshape(item_count * heads_dev, length, head_size)
        )

    offsets = (
        head_offsets.transpose(0, 2, 1).reshape(item_count * heads_dev, length).astype(jnp.float32)
    )
    heads_out = stick_blocks(
        split_heads(head_queries), split_heads(head_keys), split_heads(head_values), offsets
    )
    mean_sq = jnp.mean(heads_out * heads_out, axis=2, keepdims=True)
    normed = (heads_out * lax.rsqrt(mean_sq + eps_norm)).astype(jnp.bfloat16)
    return (
        normed.reshape(item_count, heads_dev, length, head_size)
        .transpose(0, 2, 1, 3)
        .reshape(item_count, length, feature_count)
    )


def shards(queries, key_rows, value_rows, break_offset, hidden_in, gate_weight, out_weight):
    tokens = hidden_in[0]
    gate_rows, out_cols = turned_gather((gate_weight, out_weight), "sp", (1, 0))
    gate_pre = jnp.dot(
        tokens,
        lax.all_gather(gate_rows, "dp", axis=0, tiled=True),
        preferred_element_type=jnp.float32,
    )
    gate_act = jax.nn.silu(gate_pre)
    normed = attend(
        (
            lax.all_to_all(queries, "sp", split_axis=2, concat_axis=1, tiled=True),
            lax.all_to_all(key_rows, "sp", split_axis=2, concat_axis=1, tiled=True),
            lax.all_to_all(value_rows, "sp", split_axis=2, concat_axis=1, tiled=True),
            lax.all_to_all(break_offset, "sp", split_axis=2, concat_axis=1, tiled=True),
        )
    )
    returned = lax.all_to_all(normed, "sp", split_axis=1, concat_axis=2, tiled=True)
    gated_rows = (returned[0].astype(jnp.float32) * gate_act).astype(jnp.bfloat16)
    mixed_rows = jnp.dot(
        gated_rows,
        lax.all_gather(out_cols, "dp", axis=1, tiled=True),
        preferred_element_type=jnp.float32,
    )
    return mixed_rows.astype(jnp.bfloat16)[None]


def solution(mesh):
    return jax.shard_map(
        shards,
        mesh=mesh,
        in_specs=(
            P("dp", "sp", None),
            P("dp", "sp", None),
            P("dp", "sp", None),
            P("dp", "sp", None),
            P("dp", "sp", None),
            P("dp", "sp"),
            P("sp", "dp"),
        ),
        out_specs=P("dp", "sp", None),
        check_vma=False,
    )
```

profile of v0, /device:TPU:54, one launch (start us, length us, event | category | flops | bytes accessed | tf_op | source)
XLA Modules:
  0.0 296.1 jit_solution(12190595315451277451)
XLA Ops:
  8.2 34.7 %all_gather.9 = bf16[1024,128]{1,0:T(8,128)(2,1)S(1)} all-gather(bf16[64,128]{1,0:T(8,128)(2,1)S(1)} %pad_maximum_fusion), channel_id=1, replica_groups=mesh['sp'=16,'dp'=32] {'sp'}, dimensions={0}, use_global_device_ids=true | all-gather | bytes 278528 | tf_op jit(solution)/shard_map/all_gather | solution.py:13
  45.1 8.9 %all-to-all-start.2 = ((bf16[1,128,16]{1,0,2:T(2,128)(2,1)}), bf16[1,128,16]{1,0,2:T(2,128)(2,1)S(1)}, u32[]{:S(2)}, u32[]{:S(2)}) async-start(bf16[1,128,16]{1,0,2:T(2,128)(2,1)} %copy.78), calls=%async_computation.2 | async-start | bytes 16384 | tf_op jit(solution)/shard_map/all_to_all | solution.py:110
  55.9 2.3 reduce.6
  58.9 6.1 %all-to-all-done.2 = bf16[1,128,16]{1,0,2:T(2,128)(2,1)S(1)} async-done(((bf16[1,128,16]{1,0,2:T(2,128)(2,1)}), bf16[1,128,16]{1,0,2:T(2,128)(2,1)S(1)}, u32[]{:S(2)}, u32[]{:S(2)}) %all-to-all-start.2) | async-done | bytes 4128 | tf_op jit(solution)/shard_map/all_to_all | solution.py:110
  65.1 5.9 %all-to-all-start.3 = ((bf16[16,2,4096]{2,1,0:T(2,128)(2,1)}), bf16[16,2,4096]{2,1,0:T(2,128)(2,1)S(1)}, u32[]{:S(2)}, u32[]{:S(2)}) async-start(bf16[16,2,4096]{2,1,0:T(2,128)(2,1)} %reshape.172), calls=%async_computation.3 | async-start | bytes 524288 | tf_op jit(solution)/shard_map/all_to_all | solution.py:109
  71.4 2.3 reduce.4
  74.5 11.4 %all-to-all-done.3 = bf16[16,2,4096]{2,1,0:T(2,128)(2,1)S(1)} async-done(((bf16[16,2,4096]{2,1,0:T(2,128)(2,1)}), bf16[16,2,4096]{2,1,0:T(2,128)(2,1)S(1)}, u32[]{:S(2)}, u32[]{:S(2)}) %all-to-all-start.3) | async-done | bytes 262176 | tf_op jit(solution)/shard_map/all_to_all | solution.py:109
  85.8 5.1 %all-to-all-start = ((bf16[16,2,4096]{2,1,0:T(2,128)(2,1)}), bf16[16,2,4096]{2,1,0:T(2,128)(2,1)S(1)}, u32[]{:S(2)}, u32[]{:S(2)}) async-start(bf16[16,2,4096]{2,1,0:T(2,128)(2,1)} %reshape.168), calls=%async_computation | async-start | bytes 524288 | tf_op jit(solution)/shard_map/all_to_all | solution.py:107
  91.3 2.3 reduce.5
  94.4 11.2 %all-to-all-done = bf16[16,2,4096]{2,1,0:T(2,128)(2,1)S(1)} async-done(((bf16[16,2,4096]{2,1,0:T(2,128)(2,1)}), bf16[16,2,4096]{2,1,0:T(2,128)(2,1)S(1)}, u32[]{:S(2)}, u32[]{:S(2)}) %all-to-all-start) | async-done | bytes 262176 | tf_op jit(solution)/shard_map/all_to_all | solution.py:107
  105.7 5.2 %all-to-all-start.1 = ((bf16[16,2,4096]{2,1,0:T(2,128)(2,1)}), bf16[16,2,4096]{2,1,0:T(2,128)(2,1)S(1)}, u32[]{:S(2)}, u32[]{:S(2)}) async-start(bf16[16,2,4096]{2,1,0:T(2,128)(2,1)} %reshape.170), calls=%async_computation.1 | async-start | bytes 524288 | tf_op jit(solution)/shard_map/all_to_all | solution.py:108
  114.0 11.4 %all-to-all-done.1 = bf16[16,2,4096]{2,1,0:T(2,128)(2,1)S(1)} async-done(((bf16[16,2,4096]{2,1,0:T(2,128)(2,1)}), bf16[16,2,4096]{2,1,0:T(2,128)(2,1)S(1)}, u32[]{:S(2)}, u32[]{:S(2)}) %all-to-all-start.1) | async-done | bytes 262176 | tf_op jit(solution)/shard_map/all_to_all | solution.py:108
  126.8 117.7 %while.24 = (s32[]{:T(128)}, f32[4,1,512,64]{2,3,1,0:T(8,128)}, s32[4]{0:T(128)S(1)}, bf16[1,4,512,64]{3,2,1,0:T(8,128)(2,1)}, bf16[1,2048,64]{2,1,0:T(8,128)(2,...) while((s32[]{:T(128)}, f32[4,1,512,64]{2,3,1,0:T(8,128)}, ...), condition=%wide.region_6.7_spmd, body=%wide.region_0.6_spmd.sunk | while | flops 109617680 | bytes 10642510 | solution.py:64
  131.5 9.6 %while.25 = (s32[]{:T(128)}, f32[1,512,64]{1,2,0:T(8,128)S(1)}, f32[1,512,1]{1,2,0:T(1,128)S(1)}, s32[]{:T(128)}, s32[]{:T(128)}, /*index=5*/bf16[1,2048,64]{2,1...) while((s32[]{:T(128)}, f32[1,512,64]{1,2,0:T(8,128)S(1)}, ...), condition=%wide.region_5.5_spmd.clone, body=%wide.region_1.4_spmd.clone.sunk | while | flops 109617672 | bytes 10115295 | solution.py:61
  132.1 1.9 fusion.42
  134.0 4.8 %fusion.43 = f32[1,512,4,128]{1,2,3,0:T(4,128)S(1)} fusion(f32[1,512,4,128]{1,3,2,0:T(8,128)S(1)} %bitcast.136), kind=kOutput, calls=%fused_computation.18.clone.1 | output fusion | flops 33292288 | bytes 2097152 | tf_op jit(solution)/shard_map/reduce-window
  146.5 19.2 %while.25 = (s32[]{:T(128)}, f32[1,512,64]{1,2,0:T(8,128)S(1)}, f32[1,512,1]{1,2,0:T(1,128)S(1)}, s32[]{:T(128)}, s32[]{:T(128)}, /*index=5*/bf16[1,2048,64]{2,1...) while((s32[]{:T(128)}, f32[1,512,64]{1,2,0:T(8,128)S(1)}, ...), condition=%wide.region_5.5_spmd.clone, body=%wide.region_1.4_spmd.clone.sunk | while | flops 109617672 | bytes 10115295 | solution.py:61
  149.0 4.8 %fusion.43 = f32[1,512,4,128]{1,2,3,0:T(4,128)S(1)} fusion(f32[1,512,4,128]{1,3,2,0:T(8,128)S(1)} %bitcast.136), kind=kOutput, calls=%fused_computation.18.clone.1 | output fusion | flops 33292288 | bytes 2097152 | tf_op jit(solution)/shard_map/reduce-window
  158.6 4.8 %fusion.43 = f32[1,512,4,128]{1,2,3,0:T(4,128)S(1)} fusion(f32[1,512,4,128]{1,3,2,0:T(8,128)S(1)} %bitcast.136), kind=kOutput, calls=%fused_computation.18.clone.1 | output fusion | flops 33292288 | bytes 2097152 | tf_op jit(solution)/shard_map/reduce-window
  171.1 28.9 %while.25 = (s32[]{:T(128)}, f32[1,512,64]{1,2,0:T(8,128)S(1)}, f32[1,512,1]{1,2,0:T(1,128)S(1)}, s32[]{:T(128)}, s32[]{:T(128)}, /*index=5*/bf16[1,2048,64]{2,1...) while((s32[]{:T(128)}, f32[1,512,64]{1,2,0:T(8,128)S(1)}, ...), condition=%wide.region_5.5_spmd.clone, body=%wide.region_1.4_spmd.clone.sunk | while | flops 109617672 | bytes 10115295 | solution.py:61
  173.6 4.8 %fusion.43 = f32[1,512,4,128]{1,2,3,0:T(4,128)S(1)} fusion(f32[1,512,4,128]{1,3,2,0:T(8,128)S(1)} %bitcast.136), kind=kOutput, calls=%fused_computation.18.clone.1 | output fusion | flops 33292288 | bytes 2097152 | tf_op jit(solution)/shard_map/reduce-window
  183.2 4.8 %fusion.43 = f32[1,512,4,128]{1,2,3,0:T(4,128)S(1)} fusion(f32[1,512,4,128]{1,3,2,0:T(8,128)S(1)} %bitcast.136), kind=kOutput, calls=%fused_computation.18.clone.1 | output fusion | flops 33292288 | bytes 2097152 | tf_op jit(solution)/shard_map/reduce-window
  192.8 4.8 %fusion.43 = f32[1,512,4,128]{1,2,3,0:T(4,128)S(1)} fusion(f32[1,512,4,128]{1,3,2,0:T(8,128)S(1)} %bitcast.136), kind=kOutput, calls=%fused_computation.18.clone.1 | output fusion | flops 33292288 | bytes 2097152 | tf_op jit(solution)/shard_map/reduce-window
  205.3 38.5 %while.25 = (s32[]{:T(128)}, f32[1,512,64]{1,2,0:T(8,128)S(1)}, f32[1,512,1]{1,2,0:T(1,128)S(1)}, s32[]{:T(128)}, s32[]{:T(128)}, /*index=5*/bf16[1,2048,64]{2,1...) while((s32[]{:T(128)}, f32[1,512,64]{1,2,0:T(8,128)S(1)}, ...), condition=%wide.region_5.5_spmd.clone, body=%wide.region_1.4_spmd.clone.sunk | while | flops 109617672 | bytes 10115295 | solution.py:61
  207.8 4.8 %fusion.43 = f32[1,512,4,128]{1,2,3,0:T(4,128)S(1)} fusion(f32[1,512,4,128]{1,3,2,0:T(8,128)S(1)} %bitcast.136), kind=kOutput, calls=%fused_computation.18.clone.1 | output fusion | flops 33292288 | bytes 2097152 | tf_op jit(solution)/shard_map/reduce-window
  217.5 4.8 %fusion.43 = f32[1,512,4,128]{1,2,3,0:T(4,128)S(1)} fusion(f32[1,512,4,128]{1,3,2,0:T(8,128)S(1)} %bitcast.136), kind=kOutput, calls=%fused_computation.18.clone.1 | output fusion | flops 33292288 | bytes 2097152 | tf_op jit(solution)/shard_map/reduce-window
  227.1 4.8 %fusion.43 = f32[1,512,4,128]{1,2,3,0:T(4,128)S(1)} fusion(f32[1,512,4,128]{1,3,2,0:T(8,128)S(1)} %bitcast.136), kind=kOutput, calls=%fused_computation.18.clone.1 | output fusion | flops 33292288 | bytes 2097152 | tf_op jit(solution)/shard_map/reduce-window
  236.7 4.8 %fusion.43 = f32[1,512,4,128]{1,2,3,0:T(4,128)S(1)} fusion(f32[1,512,4,128]{1,3,2,0:T(8,128)S(1)} %bitcast.136), kind=kOutput, calls=%fused_computation.18.clone.1 | output fusion | flops 33292288 | bytes 2097152 | tf_op jit(solution)/shard_map/reduce-window
  247.4 11.8 %reduce.7 = bf16[2048,64]{1,0:T(8,128)(2,1)S(1)} reduce(bf16[2048,1,64]{2,1,0:T(2,128)(2,1)S(1)} %bitcast.140, bf16[]{:T(256)} %broadcast.71), dimensions={1}, to_apply=%bitcast.94.reduce_sub_computation | reduce | bytes 524290
  259.6 20.0 %all_to_all.69 = bf16[16,2,4096]{2,1,0:T(2,128)(2,1)S(1)} all-to-all(bf16[16,2,4096]{2,1,0:T(2,128)(2,1)S(1)} %reshape.174), channel_id=1, replica_groups=mesh['sp'=16,'dp'=32] {'sp'}, dimensions={0} | all-to-all | bytes 524288 | tf_op jit(solution)/shard_map/all_to_all | solution.py:113
  281.2 3.5 %fusion.24 = bf16[128,1024]{0,1:T(8,128)(2,1)S(1)} fusion(f32[1,128,16,64]{1,3,2,0:T(8,128)S(1)} %copy.87, bf16[2048,1024]{1,0:T(8,128)(2,1)} %all-gather.3.cloned.1.call-done, bf16[1,128,2048]{2,1,0:T(8,128)(2,1)S(1)} %copy-done), kind=kOutput, calls=%fused_computation.40 | convolution fusion | flops 537657344 | bytes 5505024 | tf_op jit(solution)/shard_map/dot_general | solution.py:99
  284.7 4.5 %fusion.22 = bf16[1,128,2048]{2,1,0:T(8,128)(2,1)} fusion(bf16[128,1024]{0,1:T(8,128)(2,1)S(1)} %fusion.24, bf16[1024,2048]{0,1:T(8,128)(2,1)} %all-gather.5.cloned.1.call-done), kind=kOutput, calls=%fused_computation.36 | convolution fusion | flops 537133056 | bytes 4980736 | tf_op jit(solution)/shard_map/dot_general | solution.py:115
  (168 shorter events, 66.5 us)
Async XLA Ops:
  6.5 274.7 %copy-start = (bf16[1,128,2048]{2,1,0:T(8,128)(2,1)S(1)}, bf16[1,128,2048]{2,1,0:T(8,128)(2,1)}, u32[]{:S(2)}) copy-start(bf16[1,128,2048]{2,1,0:T(8,128)(2,1)} %param.15) | copy-start | bytes 1572868
  6.5 64.4 %copy-start.1 = (bf16[1,128,1024]{2,1,0:T(8,128)(2,1)S(1)}, bf16[1,128,1024]{2,1,0:T(8,128)(2,1)}, u32[]{:S(2)}) copy-start(bf16[1,128,1024]{2,1,0:T(8,128)(2,1)} %param.11) | copy-start | bytes 786436
  6.5 84.4 %copy-start.2 = (bf16[1,128,1024]{2,1,0:T(8,128)(2,1)S(1)}, bf16[1,128,1024]{2,1,0:T(8,128)(2,1)}, u32[]{:S(2)}) copy-start(bf16[1,128,1024]{2,1,0:T(8,128)(2,1)} %param.12) | copy-start | bytes 786436
  6.5 274.6 %all-gather.3.cloned.1.call-start = ((), (), s32[]{:S(2)}) async-start(), calls=%async_computation.5 | async-start | bytes 4325376 | tf_op jit(solution)/shard_map/all_gather | solution.py:101
  45.1 19.9 %all-to-all-start.2 = ((bf16[1,128,16]{1,0,2:T(2,128)(2,1)}), bf16[1,128,16]{1,0,2:T(2,128)(2,1)S(1)}, u32[]{:S(2)}, u32[]{:S(2)}) async-start(bf16[1,128,16]{1,0,2:T(2,128)(2,1)} %copy.78), calls=%async_computation.2 | async-start | bytes 16384 | tf_op jit(solution)/shard_map/all_to_all | solution.py:110
  65.1 20.8 %all-to-all-start.3 = ((bf16[16,2,4096]{2,1,0:T(2,128)(2,1)}), bf16[16,2,4096]{2,1,0:T(2,128)(2,1)S(1)}, u32[]{:S(2)}, u32[]{:S(2)}) async-start(bf16[16,2,4096]{2,1,0:T(2,128)(2,1)} %reshape.172), calls=%async_computation.3 | async-start | bytes 524288 | tf_op jit(solution)/shard_map/all_to_all | solution.py:109
  85.8 19.8 %all-to-all-start = ((bf16[16,2,4096]{2,1,0:T(2,128)(2,1)}), bf16[16,2,4096]{2,1,0:T(2,128)(2,1)S(1)}, u32[]{:S(2)}, u32[]{:S(2)}) async-start(bf16[16,2,4096]{2,1,0:T(2,128)(2,1)} %reshape.168), calls=%async_computation | async-start | bytes 524288 | tf_op jit(solution)/shard_map/all_to_all | solution.py:107
  105.7 19.7 %all-to-all-start.1 = ((bf16[16,2,4096]{2,1,0:T(2,128)(2,1)}), bf16[16,2,4096]{2,1,0:T(2,128)(2,1)S(1)}, u32[]{:S(2)}, u32[]{:S(2)}) async-start(bf16[16,2,4096]{2,1,0:T(2,128)(2,1)} %reshape.170), calls=%async_computation.1 | async-start | bytes 524288 | tf_op jit(solution)/shard_map/all_to_all | solution.py:108
  110.9 173.8 %all-gather.5.cloned.1.call-start = ((), (), s32[]{:S(2)}) async-start(), calls=%async_computation.6 | async-start | bytes 4325376 | tf_op jit(solution)/shard_map/all_gather | solution.py:117
Sparse Core Ops, SparseCore 0:
  44.0 56.9 all-gather.2
  114.8 60.2 all-gather.4
where the time goes:
time: 297 us; the launch traced here: 296 us
  other arithmetic  84.9 us (29%)
  blocking collectives  54.6 us (18%)
  waiting for transfers between devices  40.2 us (14%)
  matrix products  29.4 us (10%)
  local copies, waits for them, and re-layouts  28.5 us (10%)
  starting transfers between devices  25.3 us (9%)
  loops' own time  19.6 us (7%)
  between operations  13.6 us (5%)
    another operation x20, other arithmetic  48.3 us
    all_gather x1, blocking collectives, turned_gather(): out = lax.all_gather(both, axis, axis=0, tiled=True)  34.7 us
    all_to_all x1, blocking collectives, shards(): lax.all_to_all(normed, 'sp', split_axis=1, concat_axis=2, tiled=True)  20 us
    unnamed x6, other arithmetic  18.8 us
    dot_general x10, matrix products, key_step(): jnp.einsum('gqd,gkd->gqk', query_block, key_block, preferred_element_type...  18.7 us
    convert_element_type x10, other arithmetic, key_step(): weights = jnp.where(earlier, jnp.exp(jax.nn.log_sigmoid(scores) + later_s...  15.7 us
    another operation x1, loops' own time, stick_blocks(): outputs = lax.map(one_block, jnp.arange(block_count, dtype=jnp.int32))  12.5 us
    all_to_all x1, waiting for transfers between devices, shards(): lax.all_to_all(value_rows, 'sp', split_axis=2, concat_axis=1, tiled=True)  11.4 us
  transfers between devices with their start and end apart: 6, of which 4 were waited for; matrix products, arithmetic and copies ran while one was open for 46% of the time, Pallas kernels for 0%

commit v1 on v0

--- a/solution.py
+++ b/solution.py
@@ -10,7 +10,14 @@
     turned = [jnp.moveaxis(a, dim, 0) for a, dim in zip(arrays, dims)]
     widths = [t[0].size for t in turned]
     both = jnp.concatenate([t.reshape(-1, w) for t, w in zip(turned, widths)], axis=1)
-    out = lax.all_gather(both, axis, axis=0, tiled=True)
+
+    def rest_state(here_x):
+        now = jnp.stack([here_x for _ in range(lax.axis_size(axis))], axis=0)
+        y1 = lax.all_to_all(now, axis, 0, 0)
+        local_next = jnp.concatenate(y1, 0)
+        return local_next
+
+    out = rest_state(both)
     blocks = jnp.split(out, [sum(widths[:k]) for k in range(1, len(widths))], axis=1)
     return tuple(
         (

time: 297 us -> 309 us (1.040)
  the two profiles are of different devices: /device:TPU:54 before, /device:TPU:10 now
where the time goes in v1:
time: 309 us; the launch traced here: 308 us
  other arithmetic  84.9 us (27%)
  blocking collectives  57.3 us (19%)
  waiting for transfers between devices  53.2 us (17%)
  matrix products  29.4 us (10%)
  local copies, waits for them, and re-layouts  28.5 us (9%)
  starting transfers between devices  21.4 us (7%)
  loops' own time  19.6 us (6%)
  between operations  13.7 us (4%)
    another operation x20, other arithmetic  48.3 us
    all_to_all x1, blocking collectives, rest_state(): y1 = lax.all_to_all(now, axis, 0, 0)  33.4 us
    all_to_all x1, blocking collectives, shards(): lax.all_to_all(normed, 'sp', split_axis=1, concat_axis=2, tiled=True)  23.9 us
    unnamed x6, other arithmetic  18.8 us
    dot_general x10, matrix products, key_step(): jnp.einsum('gqd,gkd->gqk', query_block, key_block, preferred_element_type...  18.7 us
    all_to_all x1, waiting for transfers between devices, shards(): lax.all_to_all(key_rows, 'sp', split_axis=2, concat_axis=1, tiled=True)  16.2 us
    convert_element_type x10, other arithmetic, key_step(): weights = jnp.where(earlier, jnp.exp(jax.nn.log_sigmoid(scores) + later_s...  15.7 us
    all_to_all x1, waiting for transfers between devices, shards(): lax.all_to_all(queries, 'sp', split_axis=2, concat_axis=1, tiled=True)  14.8 us
  transfers between devices with their start and end apart: 6, of which 4 were waited for; matrix products, arithmetic and copies ran while one was open for 44% of the time, Pallas kernels for 0%

profile of v1, /device:TPU:10, one launch (start us, length us, event | category | flops | bytes accessed | tf_op | source)
XLA Modules:
  0.0 308.0 jit_solution(10103287003376177400)
XLA Ops:
  8.3 33.4 %all_to_all.74 = bf16[16,64,128]{2,1,0:T(8,128)(2,1)S(1)} all-to-all(bf16[16,64,128]{2,1,0:T(8,128)(2,1)S(1)} %stack.2), channel_id=1, replica_groups=mesh['sp'=16,'dp'=32] {'sp'}, dimensions={0} | all-to-all | bytes 524288 | tf_op jit(solution)/shard_map/all_to_all | solution.py:16
  43.9 5.8 %all-to-all-start.2 = ((bf16[1,128,16]{1,0,2:T(2,128)(2,1)}), bf16[1,128,16]{1,0,2:T(2,128)(2,1)S(1)}, u32[]{:S(2)}, u32[]{:S(2)}) async-start(bf16[1,128,16]{1,0,2:T(2,128)(2,1)} %copy.79), calls=%async_computation.2 | async-start | bytes 16384 | tf_op jit(solution)/shard_map/all_to_all | solution.py:117
  51.6 2.3 reduce.6
  54.6 7.5 %all-to-all-done.2 = bf16[1,128,16]{1,0,2:T(2,128)(2,1)S(1)} async-done(((bf16[1,128,16]{1,0,2:T(2,128)(2,1)}), bf16[1,128,16]{1,0,2:T(2,128)(2,1)S(1)}, u32[]{:S(2)}, u32[]{:S(2)}) %all-to-all-start.2) | async-done | bytes 4128 | tf_op jit(solution)/shard_map/all_to_all | solution.py:117
  62.1 4.6 %all-to-all-start.3 = ((bf16[16,2,4096]{2,1,0:T(2,128)(2,1)}), bf16[16,2,4096]{2,1,0:T(2,128)(2,1)S(1)}, u32[]{:S(2)}, u32[]{:S(2)}) async-start(bf16[16,2,4096]{2,1,0:T(2,128)(2,1)} %reshape.178), calls=%async_computation.3 | async-start | bytes 524288 | tf_op jit(solution)/shard_map/all_to_all | solution.py:116
  67.1 2.3 reduce.4
  70.2 14.7 %all-to-all-done.3 = bf16[16,2,4096]{2,1,0:T(2,128)(2,1)S(1)} async-done(((bf16[16,2,4096]{2,1,0:T(2,128)(2,1)}), bf16[16,2,4096]{2,1,0:T(2,128)(2,1)S(1)}, u32[]{:S(2)}, u32[]{:S(2)}) %all-to-all-start.3) | async-done | bytes 262176 | tf_op jit(solution)/shard_map/all_to_all | solution.py:116
  84.8 5.4 %all-to-all-start = ((bf16[16,2,4096]{2,1,0:T(2,128)(2,1)}), bf16[16,2,4096]{2,1,0:T(2,128)(2,1)S(1)}, u32[]{:S(2)}, u32[]{:S(2)}) async-start(bf16[16,2,4096]{2,1,0:T(2,128)(2,1)} %reshape.174), calls=%async_computation | async-start | bytes 524288 | tf_op jit(solution)/shard_map/all_to_all | solution.py:114
  90.6 2.3 reduce.5
  93.7 14.8 %all-to-all-done = bf16[16,2,4096]{2,1,0:T(2,128)(2,1)S(1)} async-done(((bf16[16,2,4096]{2,1,0:T(2,128)(2,1)}), bf16[16,2,4096]{2,1,0:T(2,128)(2,1)S(1)}, u32[]{:S(2)}, u32[]{:S(2)}) %all-to-all-start) | async-done | bytes 262176 | tf_op jit(solution)/shard_map/all_to_all | solution.py:114
  108.4 5.5 %all-to-all-start.1 = ((bf16[16,2,4096]{2,1,0:T(2,128)(2,1)}), bf16[16,2,4096]{2,1,0:T(2,128)(2,1)S(1)}, u32[]{:S(2)}, u32[]{:S(2)}) async-start(bf16[16,2,4096]{2,1,0:T(2,128)(2,1)} %reshape.176), calls=%async_computation.1 | async-start | bytes 524288 | tf_op jit(solution)/shard_map/all_to_all | solution.py:115
  116.2 16.2 %all-to-all-done.1 = bf16[16,2,4096]{2,1,0:T(2,128)(2,1)S(1)} async-done(((bf16[16,2,4096]{2,1,0:T(2,128)(2,1)}), bf16[16,2,4096]{2,1,0:T(2,128)(2,1)S(1)}, u32[]{:S(2)}, u32[]{:S(2)}) %all-to-all-start.1) | async-done | bytes 262176 | tf_op jit(solution)/shard_map/all_to_all | solution.py:115
  134.7 117.7 %while.24 = (s32[]{:T(128)}, f32[4,1,512,64]{2,3,1,0:T(8,128)}, s32[4]{0:T(128)S(1)}, bf16[1,4,512,64]{3,2,1,0:T(8,128)(2,1)}, bf16[1,2048,64]{2,1,0:T(8,128)(2,...) while((s32[]{:T(128)}, f32[4,1,512,64]{2,3,1,0:T(8,128)}, ...), condition=%wide.region_6.7_spmd, body=%wide.region_0.6_spmd.sunk | while | flops 109617680 | bytes 10642510 | solution.py:71
  139.4 9.6 %while.25 = (s32[]{:T(128)}, f32[1,512,64]{1,2,0:T(8,128)S(1)}, f32[1,512,1]{1,2,0:T(1,128)S(1)}, s32[]{:T(128)}, s32[]{:T(128)}, /*index=5*/bf16[1,2048,64]{2,1...) while((s32[]{:T(128)}, f32[1,512,64]{1,2,0:T(8,128)S(1)}, ...), condition=%wide.region_5.5_spmd.clone, body=%wide.region_1.4_spmd.clone.sunk | while | flops 109617672 | bytes 10115295 | solution.py:68
  142.0 4.8 %fusion.43 = f32[1,512,4,128]{1,2,3,0:T(4,128)S(1)} fusion(f32[1,512,4,128]{1,3,2,0:T(8,128)S(1)} %bitcast.137), kind=kOutput, calls=%fused_computation.18.clone.1 | output fusion | flops 33292288 | bytes 2097152 | tf_op jit(solution)/shard_map/reduce-window
  154.4 19.2 %while.25 = (s32[]{:T(128)}, f32[1,512,64]{1,2,0:T(8,128)S(1)}, f32[1,512,1]{1,2,0:T(1,128)S(1)}, s32[]{:T(128)}, s32[]{:T(128)}, /*index=5*/bf16[1,2048,64]{2,1...) while((s32[]{:T(128)}, f32[1,512,64]{1,2,0:T(8,128)S(1)}, ...), condition=%wide.region_5.5_spmd.clone, body=%wide.region_1.4_spmd.clone.sunk | while | flops 109617672 | bytes 10115295 | solution.py:68
  156.9 4.8 %fusion.43 = f32[1,512,4,128]{1,2,3,0:T(4,128)S(1)} fusion(f32[1,512,4,128]{1,3,2,0:T(8,128)S(1)} %bitcast.137), kind=kOutput, calls=%fused_computation.18.clone.1 | output fusion | flops 33292288 | bytes 2097152 | tf_op jit(solution)/shard_map/reduce-window
  166.6 4.8 %fusion.43 = f32[1,512,4,128]{1,2,3,0:T(4,128)S(1)} fusion(f32[1,512,4,128]{1,3,2,0:T(8,128)S(1)} %bitcast.137), kind=kOutput, calls=%fused_computation.18.clone.1 | output fusion | flops 33292288 | bytes 2097152 | tf_op jit(solution)/shard_map/reduce-window
  179.0 28.9 %while.25 = (s32[]{:T(128)}, f32[1,512,64]{1,2,0:T(8,128)S(1)}, f32[1,512,1]{1,2,0:T(1,128)S(1)}, s32[]{:T(128)}, s32[]{:T(128)}, /*index=5*/bf16[1,2048,64]{2,1...) while((s32[]{:T(128)}, f32[1,512,64]{1,2,0:T(8,128)S(1)}, ...), condition=%wide.region_5.5_spmd.clone, body=%wide.region_1.4_spmd.clone.sunk | while | flops 109617672 | bytes 10115295 | solution.py:68
  179.7 1.9 fusion.42
  181.6 4.8 %fusion.43 = f32[1,512,4,128]{1,2,3,0:T(4,128)S(1)} fusion(f32[1,512,4,128]{1,3,2,0:T(8,128)S(1)} %bitcast.137), kind=kOutput, calls=%fused_computation.18.clone.1 | output fusion | flops 33292288 | bytes 2097152 | tf_op jit(solution)/shard_map/reduce-window
  191.2 4.8 %fusion.43 = f32[1,512,4,128]{1,2,3,0:T(4,128)S(1)} fusion(f32[1,512,4,128]{1,3,2,0:T(8,128)S(1)} %bitcast.137), kind=kOutput, calls=%fused_computation.18.clone.1 | output fusion | flops 33292288 | bytes 2097152 | tf_op jit(solution)/shard_map/reduce-window
  200.8 4.8 %fusion.43 = f32[1,512,4,128]{1,2,3,0:T(4,128)S(1)} fusion(f32[1,512,4,128]{1,3,2,0:T(8,128)S(1)} %bitcast.137), kind=kOutput, calls=%fused_computation.18.clone.1 | output fusion | flops 33292288 | bytes 2097152 | tf_op jit(solution)/shard_map/reduce-window
  213.2 38.5 %while.25 = (s32[]{:T(128)}, f32[1,512,64]{1,2,0:T(8,128)S(1)}, f32[1,512,1]{1,2,0:T(1,128)S(1)}, s32[]{:T(128)}, s32[]{:T(128)}, /*index=5*/bf16[1,2048,64]{2,1...) while((s32[]{:T(128)}, f32[1,512,64]{1,2,0:T(8,128)S(1)}, ...), condition=%wide.region_5.5_spmd.clone, body=%wide.region_1.4_spmd.clone.sunk | while | flops 109617672 | bytes 10115295 | solution.py:68
  215.8 4.8 %fusion.43 = f32[1,512,4,128]{1,2,3,0:T(4,128)S(1)} fusion(f32[1,512,4,128]{1,3,2,0:T(8,128)S(1)} %bitcast.137), kind=kOutput, calls=%fused_computation.18.clone.1 | output fusion | flops 33292288 | bytes 2097152 | tf_op jit(solution)/shard_map/reduce-window
  225.4 4.8 %fusion.43 = f32[1,512,4,128]{1,2,3,0:T(4,128)S(1)} fusion(f32[1,512,4,128]{1,3,2,0:T(8,128)S(1)} %bitcast.137), kind=kOutput, calls=%fused_computation.18.clone.1 | output fusion | flops 33292288 | bytes 2097152 | tf_op jit(solution)/shard_map/reduce-window
  235.0 4.8 %fusion.43 = f32[1,512,4,128]{1,2,3,0:T(4,128)S(1)} fusion(f32[1,512,4,128]{1,3,2,0:T(8,128)S(1)} %bitcast.137), kind=kOutput, calls=%fused_computation.18.clone.1 | output fusion | flops 33292288 | bytes 2097152 | tf_op jit(solution)/shard_map/reduce-window
  244.6 4.8 %fusion.43 = f32[1,512,4,128]{1,2,3,0:T(4,128)S(1)} fusion(f32[1,512,4,128]{1,3,2,0:T(8,128)S(1)} %bitcast.137), kind=kOutput, calls=%fused_computation.18.clone.1 | output fusion | flops 33292288 | bytes 2097152 | tf_op jit(solution)/shard_map/reduce-window
  255.4 11.8 %reduce.7 = bf16[2048,64]{1,0:T(8,128)(2,1)S(1)} reduce(bf16[2048,1,64]{2,1,0:T(2,128)(2,1)S(1)} %bitcast.141, bf16[]{:T(256)} %broadcast.73), dimensions={1}, to_apply=%bitcast.95.reduce_sub_computation | reduce | bytes 524290
  267.6 23.9 %all_to_all.75 = bf16[16,2,4096]{2,1,0:T(2,128)(2,1)S(1)} all-to-all(bf16[16,2,4096]{2,1,0:T(2,128)(2,1)S(1)} %reshape.180), channel_id=1, replica_groups=mesh['sp'=16,'dp'=32] {'sp'}, dimensions={0} | all-to-all | bytes 524288 | tf_op jit(solution)/shard_map/all_to_all | solution.py:120
  293.1 3.5 %fusion.24 = bf16[128,1024]{0,1:T(8,128)(2,1)S(1)} fusion(f32[1,128,16,64]{1,3,2,0:T(8,128)S(1)} %copy.88, bf16[2048,1024]{1,0:T(8,128)(2,1)} %all-gather.3.cloned.1.call-done, bf16[1,128,2048]{2,1,0:T(8,128)(2,1)S(1)} %copy-done), kind=kOutput, calls=%fused_computation.40 | convolution fusion | flops 537657344 | bytes 5505024 | tf_op jit(solution)/shard_map/dot_general | solution.py:106
  296.6 4.5 %fusion.22 = bf16[1,128,2048]{2,1,0:T(8,128)(2,1)} fusion(bf16[128,1024]{0,1:T(8,128)(2,1)S(1)} %fusion.24, bf16[1024,2048]{0,1:T(8,128)(2,1)} %all-gather.5.cloned.1.call-done), kind=kOutput, calls=%fused_computation.36 | convolution fusion | flops 537133056 | bytes 4980736 | tf_op jit(solution)/shard_map/dot_general | solution.py:122
  (169 shorter events, 66.5 us)
Async XLA Ops:
  6.5 286.5 %copy-start = (bf16[1,128,2048]{2,1,0:T(8,128)(2,1)S(1)}, bf16[1,128,2048]{2,1,0:T(8,128)(2,1)}, u32[]{:S(2)}) copy-start(bf16[1,128,2048]{2,1,0:T(8,128)(2,1)} %param.15) | copy-start | bytes 1572868
  6.5 60.1 %copy-start.1 = (bf16[1,128,1024]{2,1,0:T(8,128)(2,1)S(1)}, bf16[1,128,1024]{2,1,0:T(8,128)(2,1)}, u32[]{:S(2)}) copy-start(bf16[1,128,1024]{2,1,0:T(8,128)(2,1)} %param.11) | copy-start | bytes 786436
  6.5 83.7 %copy-start.2 = (bf16[1,128,1024]{2,1,0:T(8,128)(2,1)S(1)}, bf16[1,128,1024]{2,1,0:T(8,128)(2,1)}, u32[]{:S(2)}) copy-start(bf16[1,128,1024]{2,1,0:T(8,128)(2,1)} %param.12) | copy-start | bytes 786436
  6.5 286.5 %all-gather.3.cloned.1.call-start = ((), (), s32[]{:S(2)}) async-start(), calls=%async_computation.6 | async-start | bytes 4325376 | tf_op jit(solution)/shard_map/all_gather | solution.py:108
  43.9 18.2 %all-to-all-start.2 = ((bf16[1,128,16]{1,0,2:T(2,128)(2,1)}), bf16[1,128,16]{1,0,2:T(2,128)(2,1)S(1)}, u32[]{:S(2)}, u32[]{:S(2)}) async-start(bf16[1,128,16]{1,0,2:T(2,128)(2,1)} %copy.79), calls=%async_computation.2 | async-start | bytes 16384 | tf_op jit(solution)/shard_map/all_to_all | solution.py:117
  62.1 22.7 %all-to-all-start.3 = ((bf16[16,2,4096]{2,1,0:T(2,128)(2,1)}), bf16[16,2,4096]{2,1,0:T(2,128)(2,1)S(1)}, u32[]{:S(2)}, u32[]{:S(2)}) async-start(bf16[16,2,4096]{2,1,0:T(2,128)(2,1)} %reshape.178), calls=%async_computation.3 | async-start | bytes 524288 | tf_op jit(solution)/shard_map/all_to_all | solution.py:116
  84.8 23.6 %all-to-all-start = ((bf16[16,2,4096]{2,1,0:T(2,128)(2,1)}), bf16[16,2,4096]{2,1,0:T(2,128)(2,1)S(1)}, u32[]{:S(2)}, u32[]{:S(2)}) async-start(bf16[16,2,4096]{2,1,0:T(2,128)(2,1)} %reshape.174), calls=%async_computation | async-start | bytes 524288 | tf_op jit(solution)/shard_map/all_to_all | solution.py:114
  108.4 24.0 %all-to-all-start.1 = ((bf16[16,2,4096]{2,1,0:T(2,128)(2,1)}), bf16[16,2,4096]{2,1,0:T(2,128)(2,1)S(1)}, u32[]{:S(2)}, u32[]{:S(2)}) async-start(bf16[16,2,4096]{2,1,0:T(2,128)(2,1)} %reshape.176), calls=%async_computation.1 | async-start | bytes 524288 | tf_op jit(solution)/shard_map/all_to_all | solution.py:115
  113.9 182.7 %all-gather.5.cloned.1.call-start = ((), (), s32[]{:S(2)}) async-start(), calls=%async_computation.7 | async-start | bytes 4325376 | tf_op jit(solution)/shard_map/all_gather | solution.py:124
Sparse Core Ops, SparseCore 0:
  42.7 54.7 all-gather.2
  134.8 54.5 all-gather.4
